TPU v7x, 512 devices: a whole 4x4x16 slice. The times are simulated.
512 devices in a mesh: fs: 64 (over z, y), tp: 8 (over x, core).
Axes of the slice: x: 4, y: 4, z: 16, core: 2. Of those that a mesh axis runs over, the one named last changes fastest.
Arguments:
- tokens: bfloat16 [24576, 2048], P('fs'), may hold values from -6 to 6
- merged: bfloat16 [24576, 2048], P('fs'), may hold values from -6 to 6
- gain_first: float32 [2048], replicated, may hold values from 0.1 to 1.9
- gate_first: bfloat16 [2048, 2816], P('fs', 'tp'), may hold values from -0.125 to 0.125
- up_first: bfloat16 [2048, 2816], P('fs', 'tp'), may hold values from -0.125 to 0.125
- down_first: bfloat16 [2816, 2048], P('tp', 'fs'), may hold values from -0.21875 to 0.21875
- gain_second: float32 [2048], replicated, may hold values from 0.1 to 1.9
- gate_second: bfloat16 [2048, 2816], P('fs', 'tp'), may hold values from -0.125 to 0.125
- up_second: bfloat16 [2048, 2816], P('fs', 'tp'), may hold values from -0.125 to 0.125
- down_second: bfloat16 [2816, 2048], P('tp', 'fs'), may hold values from -0.21875 to 0.21875
Outputs:
- result: bfloat16 [24576, 2048], P('fs')
All inputs are finite; a program needn't handle non-finite values.
Results may differ from a plain program's by a relative error of at most 0.01.
Values may be sent and summed in bfloat16 or wider, within the bound.
No kernel may reach another device: no remote copies, remote signals or barrier semaphores. Data moves between devices by JAX's collectives and lax.ppermute only.
A program may use at most 64 MiB of HBM per device.

v0:
```python
import jax
import jax.numpy as jnp
from jax import lax
from jax.sharding import Mesh
from jax.sharding import PartitionSpec as P

FS = ("z", "y")
TP = ("x", "c")
EPS = 1e-06
NZ, NY, NX, NC = 16, 4, 4, 2

W_SCALE = 2.0**18
A_SCALE = 2.0**8


def norm_rows(values, gain):
    scale = lax.rsqrt(jnp.mean(values * values, axis=-1, keepdims=True) + EPS)
    return values * scale * gain


def swap_cores(x):
    return lax.ppermute(x, "c", [(0, 1), (1, 0)])


def half_coded(w):
    return (w.astype(jnp.float32) * W_SCALE).astype(jnp.float16)


def plain(w):
    return (w.astype(jnp.float32) * (1.0 / W_SCALE)).astype(jnp.bfloat16)


def gather_weights(first, second):
    count, rows, width = second.shape
    padded = jnp.pad(second.reshape(count * rows, width), ((0, (NY - 1) * count * rows), (0, 0)))
    padded, first = lax.optimization_barrier((padded, first))
    second_y = lax.all_gather(padded, "y", axis=0, tiled=True)
    first_z = lax.all_gather(first, "z", axis=0)
    second_y, first_z = lax.optimization_barrier((second_y, first_z))
    block = second_y.reshape(NY, -1, width)[:, : count * rows].reshape(NY * count * rows, width)
    block, first_z = lax.optimization_barrier((block, first_z))
    second_whole = lax.all_gather(block, "z", axis=0, tiled=True).reshape(NZ, NY, count, rows, width)
    first_whole = lax.all_gather(first_z, "y", axis=1)
    return [[plain(first_whole[:, :, k]).reshape(-1, width) for k in range(count)], [second_whole[:, :, k].reshape(-1, width) for k in range(count)]]


def folded(normed, gate_w, up_w):
    gate = jnp.dot(normed, gate_w, preferred_element_type=jnp.float32)
    up = jnp.dot(normed, up_w, preferred_element_type=jnp.float32)
    return (jax.nn.silu(gate) * up).astype(jnp.bfloat16)


def down_dot(hidden, down_t):
    return lax.dot_general(hidden, down_t, (((1,), (1,)), ((), ())), preferred_element_type=jnp.float32)


def summed_at_owner(hidden, down_t, share):
    core = lax.axis_index("c")
    parts = hidden.reshape(NX, NC, share, hidden.shape[-1])
    other = lax.dynamic_index_in_dim(parts, 1 - core, 1, keepdims=False).reshape(NX * share, -1)
    mine = lax.dynamic_index_in_dim(parts, core, 1, keepdims=False).reshape(NX * share, -1)
    sent = swap_cores(down_dot(other, down_t).astype(jnp.bfloat16))
    chip = (down_dot(mine, down_t) + sent.astype(jnp.float32)).astype(jnp.bfloat16)
    pieces = lax.all_to_all(chip.reshape(NX, share, -1), "x", 0, 0, tiled=True)
    return jnp.sum(pieces.astype(jnp.float32), axis=0)


def body(tokens, merged, gain_first, gate_first, up_first, down_first, gain_second, gate_second, up_second, down_second):
    rows = tokens.shape[0]
    share = rows // (NX * NC)
    core = lax.axis_index("c")
    offset = (lax.axis_index("x") * NC + core) * share
    own_first = jnp.stack([half_coded(w) for w in (gate_first, up_first, down_first.T)])
    first, second = gather_weights(own_first, jnp.stack((gate_second, up_second, down_second.T)))
    normed_first = norm_rows(tokens.astype(jnp.float32), gain_first).astype(jnp.bfloat16)
    hidden = folded(normed_first, first[0], first[1])
    first_sum = summed_at_owner(hidden, first[2], share)
    base = lax.dynamic_slice_in_dim(tokens, offset, share, 0).astype(jnp.float32)
    extra = lax.dynamic_slice_in_dim(merged, offset, share, 0).astype(jnp.float32)
    middle = base + extra + 0.5 * first_sum
    normed_share = norm_rows(middle, gain_second).astype(jnp.bfloat16)
    coded = (normed_share.astype(jnp.float32) * A_SCALE).astype(jnp.float16)
    everyone = lax.all_gather(coded, TP, axis=0, tiled=True)
    normed_second = (everyone.astype(jnp.float32) * (1.0 / A_SCALE)).astype(jnp.bfloat16)
    hidden_two = folded(normed_second, second[0], second[1])
    second_sum = summed_at_owner(hidden_two, second[2], share)
    finished = (middle + 0.5 * second_sum).astype(jnp.bfloat16)
    mine = lax.all_gather(finished, "x", axis=0)
    theirs = swap_cores(mine)
    low = jnp.where(core == 0, mine, theirs)
    high = jnp.where(core == 0, theirs, mine)
    return jnp.stack([low, high], axis=1).reshape(rows, -1)


def solution(mesh):
    finer = Mesh(mesh.devices.reshape(NZ, NY, NX, NC), ("z", "y", "x", "c"))
    return jax.shard_map(
        body,
        mesh=finer,
        in_specs=(P(FS, None), P(FS, None), P(), P(FS, TP), P(FS, TP), P(TP, FS), P(), P(FS, TP), P(FS, TP), P(TP, FS)),
        out_specs=P(FS, None),
        check_vma=False,
    )
```

profile of v0, /device:TPU:1, one launch (start us, length us, event | category | flops | bytes accessed | tf_op | source)
XLA Modules:
  0.0 191.4 jit_solution(12982239111705080344)
XLA Ops:
  6.5 0.0 all-gather.9.cloned.1.call-start
  6.5 0.7 fusion.13
  7.3 0.8 pad_maximum_fusion.1
  8.1 0.0 copy-start
  8.1 0.7 pad.4
  8.8 0.8 fusion.11
  9.6 0.0 all-gather.9.cloned.1.call-update
  9.7 0.0 all-gather.11.cloned.1.call-start
  9.7 37.6 %all-gather.12 = f16[48,32,352]{2,1,0:T(8,128)(2,1)S(1)} all-gather(f16[3,32,352]{2,1,0:T(8,128)(2,1)S(1)} %pad_maximum_fusion.2), channel_id=2, replica_groups=mesh['z'=16,'y'=4,'x'=4,'c'=2] {'z'}, dimensions={0}, use_global_device_ids=true | all-gather | bytes 1148928 | tf_op jit(solution)/shard_map/all_gather | solution.py:38
  47.3 0.0 all-gather.9.cloned.1.call-done
  47.3 1.7 slice.28
  49.0 0.0 all-gather.11.cloned.1.call-update
  49.0 0.0 copy-done
  49.0 0.4 fusion
  49.4 35.3 %all-gather.13 = f16[16,12,32,352]{3,2,1,0:T(8,128)(2,1)S(1)} all-gather(f16[16,3,32,352]{3,2,1,0:T(8,128)(2,1)S(1)} %bitcast.59), channel_id=3, replica_groups=mesh['z'=16,'y'=4,'x'=4,'c'=2] {'y'}, dimensions={1}, use_global_device_ids=true | all-gather | bytes 5406720 | tf_op jit(solution)/shard_map/all_gather | solution.py:43
  84.7 0.0 copy-start.2
  84.7 1.1 multiply_convert_fusion.1
  85.8 0.0 copy-done.2
  85.9 1.1 fusion.9
  86.9 1.8 fusion.6
  88.7 1.2 copy.15
  89.9 0.7 convolution_convert_fusion.1
  90.6 9.5 %collective-permute-start = (bf16[192,2048]{1,0:T(8,128)(2,1)S(1)}, bf16[192,2048]{1,0:T(8,128)(2,1)S(1)}, u32[]{:S(2)}, u32[]{:S(2)}) collective-permute-start(bf16[192,2048]{1,0:T(8,128)(2,1)S(1)} %convolution_convert_fusion.1), channel_id=1, source_target_pairs={{0,1},{1,0},{2,3},{3,2},{4,5},{5,4},{6,7},{7,6},{8,9},{9,8},{10,11... | collective-permute-start | bytes 2359304 | tf_op jit(solution)/shard_map/ppermute | solution.py:22
  100.2 1.9 collective-permute-done
  102.1 1.6 add_convert_fusion.1
  103.7 4.0 %all-to-all-start = ((bf16[4,48,2048]{2,1,0:T(8,128)(2,1)}), bf16[4,48,2048]{2,1,0:T(8,128)(2,1)S(1)}, u32[]{:S(2)}, u32[]{:S(2)}) async-start(bf16[4,48,2048]{2,1,0:T(8,128)(2,1)} %bitcast.19), calls=%async_computation | async-start | bytes 1572864 | tf_op jit(solution)/shard_map/all_to_all | solution.py:64
  107.7 0.0 copy-start.1
  107.7 11.7 %all-to-all-done = bf16[4,48,2048]{2,1,0:T(8,128)(2,1)S(1)} async-done(((bf16[4,48,2048]{2,1,0:T(8,128)(2,1)}), bf16[4,48,2048]{2,1,0:T(8,128)(2,1)S(1)}, u32[]{:S(2)}, u32[]{:S(2)}) %all-to-all-start) | async-done | bytes 786464 | tf_op jit(solution)/shard_map/all_to_all | solution.py:64
  119.4 0.1 convert_reduce_fusion.1
  119.5 1.1 multiply_reduce_fusion
  120.7 0.0 copy-done.1
  120.7 0.1 multiply_convert_fusion.10
  120.8 16.1 %all-gather.14 = f16[384,2048]{1,0:T(8,128)(2,1)S(1)} all-gather(f16[48,2048]{1,0:T(8,128)(2,1)S(1)} %multiply_convert_fusion.10), channel_id=1, replica_groups=mesh['z'=16,'y'=4,'x'=4,'c'=2] {'x','c'}, dimensions={0}, use_global_device_ids=true | all-gather | bytes 1769472 | tf_op jit(solution)/shard_map/all_gather | solution.py:83
  136.9 2.9 %fusion.16 = (bf16[16,4,1,32,352]{4,3,2,1,0:T(8,128)(2,1)S(1)}, bf16[16,4,1,32,352]{4,3,2,1,0:T(8,128)(2,1)S(1)}, bf16[16,4,1,32,352]{4,3,2,1,0:T(8,128)(2,1)S(1)}) fusion(bf16[16,4,3,32,352]{4,3,2,1,0:T(8,128)(2,1)} %bitcast.58), kind=kLoop, calls=%fused_computation.46 | loop fusion | bytes 8650752 | tf_op jit(solution)/shard_map/slice | solution.py:44
  139.9 1.0 fusion.4
  140.8 1.7 fusion.7
  142.5 1.2 copy.16
  143.7 0.7 convolution_convert_fusion
  144.5 2.1 %collective-permute-start.1 = (bf16[192,2048]{1,0:T(8,128)(2,1)S(1)}, bf16[192,2048]{1,0:T(8,128)(2,1)S(1)}, u32[]{:S(2)}, u32[]{:S(2)}) collective-permute-start(bf16[192,2048]{1,0:T(8,128)(2,1)S(1)} %convolution_convert_fusion), channel_id=1, source_target_pairs={{0,1},{1,0},{2,3},{3,2},{4,5},{5,4},{6,7},{7,6},{8,9},{9,8},{10,11... | collective-permute-start | bytes 2359304 | tf_op jit(solution)/shard_map/ppermute | solution.py:22
  146.5 2.1 %collective-permute-done.1 = bf16[192,2048]{1,0:T(8,128)(2,1)S(1)} collective-permute-done((bf16[192,2048]{1,0:T(8,128)(2,1)S(1)}, bf16[192,2048]{1,0:T(8,128)(2,1)S(1)}, u32[]{:S(2)}, u32[]{:S(2)}) %collective-permute-start.1) | collective-permute-done | bytes 786464 | tf_op jit(solution)/shard_map/ppermute | solution.py:22
  148.7 0.7 add_convert_fusion
  149.4 14.5 %all_to_all.10 = bf16[4,48,2048]{2,1,0:T(8,128)(2,1)S(1)} all-to-all(bf16[4,48,2048]{2,1,0:T(8,128)(2,1)S(1)} %bitcast.60), channel_id=1, replica_groups=mesh['z'=16,'y'=4,'x'=4,'c'=2] {'x'}, dimensions={0} | all-to-all | bytes 1572864 | tf_op jit(solution)/shard_map/all_to_all | solution.py:64
  163.9 0.1 convert_reduce_fusion
  164.1 10.9 %all-gather.2 = bf16[192,2048]{1,0:T(8,128)(2,1)S(1)} all-gather(bf16[48,2048]{1,0:T(8,128)(2,1)S(1)} %add_convert_fusion.2), channel_id=4, replica_groups=mesh['z'=16,'y'=4,'x'=4,'c'=2] {'x'}, dimensions={0}, use_global_device_ids=true | all-gather | bytes 983040 | tf_op jit(solution)/shard_map/all_gather | solution.py:88
  175.0 6.3 %collective-permute-start.2 = (bf16[4,48,2048]{2,1,0:T(8,128)(2,1)S(1)}, bf16[4,48,2048]{2,1,0:T(8,128)(2,1)S(1)}, u32[]{:S(2)}, u32[]{:S(2)}) collective-permute-start(bf16[4,48,2048]{2,1,0:T(8,128)(2,1)S(1)} %bitcast.61), channel_id=1, source_target_pairs={{0,1},{1,0},{2,3},{3,2},{4,5},{5,4},{6,7},{7,6},{8,9},{9,8},{10,11... | collective-permute-start | bytes 2359304 | tf_op jit(solution)/shard_map/ppermute | solution.py:22
  181.3 1.9 collective-permute-done.2
  183.2 0.1 select_bitcast_fusion.1
  183.3 1.3 pad_maximum_fusion
  (7 shorter events, 0.2 us)
Async XLA Ops:
  6.5 40.7 %all-gather.9.cloned.1.call-start = ((), (), s32[]{:S(2)}) async-start(), calls=%async_computation.2 | async-start | bytes 1474560 | tf_op jit(solution)/shard_map/all_gather | solution.py:37
  8.1 40.9 %copy-start = (bf16[384,2048]{1,0:T(8,128)(2,1)S(1)}, bf16[384,2048]{1,0:T(8,128)(2,1)}, u32[]{:S(2)}) copy-start(bf16[384,2048]{1,0:T(8,128)(2,1)} %param.10) | copy-start | bytes 4718596
  9.7 127.3 %all-gather.11.cloned.1.call-start = ((), (), s32[]{:S(2)}) async-start(), calls=%async_computation.3 | async-start | bytes 5013504 | tf_op jit(solution)/shard_map/all_gather | solution.py:42
  84.7 1.2 copy-start.2
  90.6 11.4 %collective-permute-start = (bf16[192,2048]{1,0:T(8,128)(2,1)S(1)}, bf16[192,2048]{1,0:T(8,128)(2,1)S(1)}, u32[]{:S(2)}, u32[]{:S(2)}) collective-permute-start(bf16[192,2048]{1,0:T(8,128)(2,1)S(1)} %convolution_convert_fusion.1), channel_id=1, source_target_pairs={{0,1},{1,0},{2,3},{3,2},{4,5},{5,4},{6,7},{7,6},{8,9},{9,8},{10,11... | collective-permute-start | bytes 2359304 | tf_op jit(solution)/shard_map/ppermute | solution.py:22
  103.7 15.7 %all-to-all-start = ((bf16[4,48,2048]{2,1,0:T(8,128)(2,1)}), bf16[4,48,2048]{2,1,0:T(8,128)(2,1)S(1)}, u32[]{:S(2)}, u32[]{:S(2)}) async-start(bf16[4,48,2048]{2,1,0:T(8,128)(2,1)} %bitcast.19), calls=%async_computation | async-start | bytes 1572864 | tf_op jit(solution)/shard_map/all_to_all | solution.py:64
  107.7 13.0 %copy-start.1 = (f32[2048]{0:T(1024)S(1)}, f32[2048]{0:T(1024)}, u32[]{:S(2)}) copy-start(f32[2048]{0:T(1024)} %param.16) | copy-start | bytes 24580
  144.5 4.2 %collective-permute-start.1 = (bf16[192,2048]{1,0:T(8,128)(2,1)S(1)}, bf16[192,2048]{1,0:T(8,128)(2,1)S(1)}, u32[]{:S(2)}, u32[]{:S(2)}) collective-permute-start(bf16[192,2048]{1,0:T(8,128)(2,1)S(1)} %convolution_convert_fusion), channel_id=1, source_target_pairs={{0,1},{1,0},{2,3},{3,2},{4,5},{5,4},{6,7},{7,6},{8,9},{9,8},{10,11... | collective-permute-start | bytes 2359304 | tf_op jit(solution)/shard_map/ppermute | solution.py:22
  175.0 8.2 %collective-permute-start.2 = (bf16[4,48,2048]{2,1,0:T(8,128)(2,1)S(1)}, bf16[4,48,2048]{2,1,0:T(8,128)(2,1)S(1)}, u32[]{:S(2)}, u32[]{:S(2)}) collective-permute-start(bf16[4,48,2048]{2,1,0:T(8,128)(2,1)S(1)} %bitcast.61), channel_id=1, source_target_pairs={{0,1},{1,0},{2,3},{3,2},{4,5},{5,4},{6,7},{7,6},{8,9},{9,8},{10,11... | collective-permute-start | bytes 2359304 | tf_op jit(solution)/shard_map/ppermute | solution.py:22
Sparse Core Ops, SparseCore 0:
  9.8 35.3 all-gather.8
  49.1 72.5 all-gather.10
where the time goes:
time: 192 us; the launch traced here: 191 us
  blocking collectives  114 us (59%)
  starting transfers between devices  21.9 us (11%)
  waiting for transfers between devices  17.6 us (9%)
  between operations  13.6 us (7%)
  matrix products  9.26 us (5%)
  local copies, waits for them, and re-layouts  7.79 us (4%)
  other arithmetic  6.84 us (4%)
    all_gather x1, blocking collectives, gather_weights(): first_z = lax.all_gather(first, 'z', axis=0)  37.6 us
    all_gather x1, blocking collectives, gather_weights(): first_whole = lax.all_gather(first_z, 'y', axis=1)  35.3 us
    ppermute x3, starting transfers between devices, swap_cores(): return lax.ppermute(x, 'c', [(0, 1), (1, 0)])  17.9 us
    all_gather x1, blocking collectives, body(): everyone = lax.all_gather(coded, TP, axis=0, tiled=True)  16.1 us
    all_to_all x1, blocking collectives, summed_at_owner(): pieces = lax.all_to_all(chip.reshape(NX, share, -1), 'x', 0, 0, tiled=True)  14.5 us
    all_to_all x1, waiting for transfers between devices, summed_at_owner(): pieces = lax.all_to_all(chip.reshape(NX, share, -1), 'x', 0, 0, tiled=True)  11.7 us
    all_gather x1, blocking collectives, body(): mine = lax.all_gather(finished, 'x', axis=0)  10.9 us
    ppermute x3, waiting for transfers between devices, swap_cores(): return lax.ppermute(x, 'c', [(0, 1), (1, 0)])  5.88 us
  transfers between devices with their start and end apart: 6, of which 4 were waited for; matrix products, arithmetic and copies ran while one was open for 5% of the time, Pallas kernels for 0%

commit v1 on v0

--- a/solution.py
+++ b/solution.py
@@ -22,6 +22,11 @@
     return lax.ppermute(x, "c", [(0, 1), (1, 0)])
 
 
+def side_by_side(mats):
+    room = -mats[0].shape[1] % 128
+    return jnp.concatenate([jnp.pad(m, ((0, 0), (0, room))) for m in mats], axis=1)
+
+
 def half_coded(w):
     return (w.astype(jnp.float32) * W_SCALE).astype(jnp.float16)
 
@@ -31,17 +36,22 @@
 
 
 def gather_weights(first, second):
-    count, rows, width = second.shape
-    padded = jnp.pad(second.reshape(count * rows, width), ((0, (NY - 1) * count * rows), (0, 0)))
+    rows, width = second.shape
+    padded = jnp.pad(second, ((0, (NY - 1) * rows), (0, 0)))
     padded, first = lax.optimization_barrier((padded, first))
     second_y = lax.all_gather(padded, "y", axis=0, tiled=True)
-    first_z = lax.all_gather(first, "z", axis=0)
+    first_z = lax.all_gather(first, "z", axis=0, tiled=True)
     second_y, first_z = lax.optimization_barrier((second_y, first_z))
-    block = second_y.reshape(NY, -1, width)[:, : count * rows].reshape(NY * count * rows, width)
+    block = second_y.reshape(NY, -1, width)[:, :rows].reshape(NY * rows, width)
     block, first_z = lax.optimization_barrier((block, first_z))
-    second_whole = lax.all_gather(block, "z", axis=0, tiled=True).reshape(NZ, NY, count, rows, width)
-    first_whole = lax.all_gather(first_z, "y", axis=1)
-    return [[plain(first_whole[:, :, k]).reshape(-1, width) for k in range(count)], [second_whole[:, :, k].reshape(-1, width) for k in range(count)]]
+    second_whole = lax.all_gather(block, "z", axis=0, tiled=True)
+    first_whole = lax.all_gather(first_z.reshape(NZ, rows, width), "y", axis=1, tiled=True)
+    return plain(first_whole.reshape(-1, width)), second_whole
+
+
+def thirds(whole):
+    width = whole.shape[1] // 3
+    return [whole[:, k * width : (k + 1) * width] for k in range(3)]
 
 
 def folded(normed, gate_w, up_w):
@@ -54,14 +64,17 @@
     return lax.dot_general(hidden, down_t, (((1,), (1,)), ((), ())), preferred_element_type=jnp.float32)
 
 
-def summed_at_owner(hidden, down_t, share):
+def pieces_at_owner(hidden, down_t, share):
     core = lax.axis_index("c")
     parts = hidden.reshape(NX, NC, share, hidden.shape[-1])
     other = lax.dynamic_index_in_dim(parts, 1 - core, 1, keepdims=False).reshape(NX * share, -1)
     mine = lax.dynamic_index_in_dim(parts, core, 1, keepdims=False).reshape(NX * share, -1)
     sent = swap_cores(down_dot(other, down_t).astype(jnp.bfloat16))
     chip = (down_dot(mine, down_t) + sent.astype(jnp.float32)).astype(jnp.bfloat16)
-    pieces = lax.all_to_all(chip.reshape(NX, share, -1), "x", 0, 0, tiled=True)
+    return lax.all_to_all(chip.reshape(NX, share, -1), "x", 0, 0, tiled=True)
+
+
+def added(pieces):
     return jnp.sum(pieces.astype(jnp.float32), axis=0)
 
 
@@ -70,11 +83,15 @@
     share = rows // (NX * NC)
     core = lax.axis_index("c")
     offset = (lax.axis_index("x") * NC + core) * share
-    own_first = jnp.stack([half_coded(w) for w in (gate_first, up_first, down_first.T)])
-    first, second = gather_weights(own_first, jnp.stack((gate_second, up_second, down_second.T)))
+    offset, tokens = lax.optimization_barrier((offset, tokens))
+    own_first = half_coded(side_by_side((gate_first, up_first, down_first.T)))
+    own_second = side_by_side((gate_second, up_second, down_second.T))
+    first, second = (thirds(whole) for whole in gather_weights(own_first, own_second))
     normed_first = norm_rows(tokens.astype(jnp.float32), gain_first).astype(jnp.bfloat16)
     hidden = folded(normed_first, first[0], first[1])
-    first_sum = summed_at_owner(hidden, first[2], share)
+    pieces = pieces_at_owner(hidden, first[2], share)
+    pieces, tokens, merged, gain_second, offset = lax.optimization_barrier((pieces, tokens, merged, gain_second, offset))
+    first_sum = added(pieces)
     base = lax.dynamic_slice_in_dim(tokens, offset, share, 0).astype(jnp.float32)
     extra = lax.dynamic_slice_in_dim(merged, offset, share, 0).astype(jnp.float32)
     middle = base + extra + 0.5 * first_sum
@@ -83,7 +100,7 @@
     everyone = lax.all_gather(coded, TP, axis=0, tiled=True)
     normed_second = (everyone.astype(jnp.float32) * (1.0 / A_SCALE)).astype(jnp.bfloat16)
     hidden_two = folded(normed_second, second[0], second[1])
-    second_sum = summed_at_owner(hidden_two, second[2], share)
+    second_sum = added(pieces_at_owner(hidden_two, second[2], share))
     finished = (middle + 0.5 * second_sum).astype(jnp.bfloat16)
     mine = lax.all_gather(finished, "x", axis=0)
     theirs = swap_cores(mine)

time: 192 us -> 185 us (0.964)
  blocking collectives: 114 us -> 130 us
  waiting for transfers between devices: 17.6 us -> 5.91 us
  local copies, waits for them, and re-layouts: 7.79 us -> 2.82 us
  starting transfers between devices: 21.9 us -> 17.8 us
    all_to_all x1 -> x2, blocking collectives: 14.5 us -> 29.8 us  [pieces_at_owner(): return lax.all_to_all(chip.reshape(NX, share, -1), 'x', 0, 0, tiled=True)]
    all_to_all x1 -> x0, waiting for transfers between devices: 11.7 us -> none  [summed_at_owner(): pieces = lax.all_to_all(chip.reshape(NX, share, -1), 'x', 0, 0, tiled=True)]
    all_to_all x1 -> x0, starting transfers between devices: 4 us -> none  [summed_at_owner(): pieces = lax.all_to_all(chip.reshape(NX, share, -1), 'x', 0, 0, tiled=True)]
    slice x2 -> x1, local copies, waits for them, and re-layouts: 4.63 us -> 1.7 us  [gather_weights(): block = second_y.reshape(NY, -1, width)[:, :rows].reshape(NY * rows, width)]
    another operation x4 -> x0, other arithmetic: 2.34 us -> none  [the longest x3 1.54 us: body(): jnp.stack([half_coded(w) for w in (gate_first, up_first, down_first.T)])]
    convert_element_type x2 -> x0, local copies, waits for them, and re-layouts: 2.32 us -> none  [folded(): return (jax.nn.silu(gate) * up).astype(jnp.bfloat16)]
  transfers between devices with their start and end apart: 6 -> 5, of which waited for: 4 -> 3; matrix products, arithmetic and copies ran while one was open for 5% -> 4% of each run, Pallas kernels for 0% -> 0%
where the time goes in v1:
time: 185 us
  blocking collectives  130 us (70%)
  starting transfers between devices  17.8 us (10%)
  between operations  13.6 us (7%)
  matrix products  8.45 us (5%)
  other arithmetic  6.34 us (3%)
  waiting for transfers between devices  5.91 us (3%)
  local copies, waits for them, and re-layouts  2.82 us (2%)
    all_gather x1, blocking collectives, gather_weights(): first_z = lax.all_gather(first, 'z', axis=0, tiled=True)  37.7 us
    all_gather x1, blocking collectives, gather_weights(): lax.all_gather(first_z.reshape(NZ, rows, width), 'y', axis=1, tiled=True)  35.4 us
    all_to_all x2, blocking collectives, pieces_at_owner(): return lax.all_to_all(chip.reshape(NX, share, -1), 'x', 0, 0, tiled=True)  29.8 us
    ppermute x3, starting transfers between devices, swap_cores(): return lax.ppermute(x, 'c', [(0, 1), (1, 0)])  17.8 us
    all_gather x1, blocking collectives, body(): everyone = lax.all_gather(coded, TP, axis=0, tiled=True)  16.4 us
    all_gather x1, blocking collectives, body(): mine = lax.all_gather(finished, 'x', axis=0)  10.9 us
    ppermute x3, waiting for transfers between devices, swap_cores(): return lax.ppermute(x, 'c', [(0, 1), (1, 0)])  5.88 us
  transfers between devices with their start and end apart: 5, of which 3 were waited for; matrix products, arithmetic and copies ran while one was open for 4% of the time, Pallas kernels for 0%

profile of v1, /device:TPU:1, one launch (start us, length us, event | category | flops | bytes accessed | tf_op | source)
XLA Modules:
  0.0 185.0 jit_solution(11697747936566345728)
XLA Ops:
  6.5 0.0 copy-start
  6.5 0.0 all-gather.7.cloned.1.call-start
  6.5 0.9 fusion.43
  7.4 0.7 pad.26
  8.2 0.8 multiply_convert_fusion.10
  9.0 0.0 all-gather.7.cloned.1.call-update
  9.0 0.0 all-gather.9.cloned.1.call-start
  9.1 37.7 %all-gather.10 = f16[512,1152]{1,0:T(8,128)(2,1)S(1)} all-gather(f16[32,1152]{1,0:T(8,128)(2,1)S(1)} %multiply_convert_fusion.10), channel_id=1, replica_groups=mesh['z'=16,'y'=4,'x'=4,'c'=2] {'z'}, dimensions={0}, use_global_device_ids=true | all-gather | bytes 1253376 | tf_op jit(solution)/shard_map/all_gather | solution.py:43
  46.7 0.0 all-gather.7.cloned.1.call-done
  46.7 1.7 slice.28
  48.4 0.0 all-gather.9.cloned.1.call-update
  48.5 0.0 copy-done
  48.5 0.4 fusion
  48.9 35.4 %all-gather.11 = f16[16,128,1152]{2,1,0:T(8,128)(2,1)S(1)} all-gather(f16[16,32,1152]{2,1,0:T(8,128)(2,1)S(1)} %bitcast.30), channel_id=1, replica_groups=mesh['z'=16,'y'=4,'x'=4,'c'=2] {'y'}, dimensions={1}, use_global_device_ids=true | all-gather | bytes 5898240 | tf_op jit(solution)/shard_map/all_gather | solution.py:48
  84.2 0.0 copy-start.3
  84.2 1.2 multiply_convert_fusion
  85.4 0.0 copy-done.3
  85.5 1.0 fusion.9
  86.5 1.1 fusion.27
  87.6 0.7 convolution_convert_fusion.1
  88.3 9.4 %collective-permute-start = (bf16[192,2048]{1,0:T(8,128)(2,1)S(1)}, bf16[192,2048]{1,0:T(8,128)(2,1)S(1)}, u32[]{:S(2)}, u32[]{:S(2)}) collective-permute-start(bf16[192,2048]{1,0:T(8,128)(2,1)S(1)} %convolution_convert_fusion.1), channel_id=1, source_target_pairs={{0,1},{1,0},{2,3},{3,2},{4,5},{5,4},{6,7},{7,6},{8,9},{9,8},{10,11... | collective-permute-start | bytes 2359304 | tf_op jit(solution)/shard_map/ppermute | solution.py:22
  97.7 1.9 %collective-permute-done = bf16[192,2048]{1,0:T(8,128)(2,1)S(1)} collective-permute-done((bf16[192,2048]{1,0:T(8,128)(2,1)S(1)}, bf16[192,2048]{1,0:T(8,128)(2,1)S(1)}, u32[]{:S(2)}, u32[]{:S(2)}) %collective-permute-start) | collective-permute-done | bytes 786464 | tf_op jit(solution)/shard_map/ppermute | solution.py:22
  99.6 0.7 add_convert_fusion.1
  100.4 15.3 %all_to_all.10 = bf16[4,48,2048]{2,1,0:T(8,128)(2,1)S(1)} all-to-all(bf16[4,48,2048]{2,1,0:T(8,128)(2,1)S(1)} %bitcast.31), channel_id=1, replica_groups=mesh['z'=16,'y'=4,'x'=4,'c'=2] {'x'}, dimensions={0} | all-to-all | bytes 1572864 | tf_op jit(solution)/shard_map/all_to_all | solution.py:74
  115.6 0.0 copy-start.2
  115.6 0.1 convert_reduce_fusion.1
  115.7 1.2 multiply_reduce_fusion
  117.0 0.0 copy-done.2
  117.0 0.1 multiply_convert_fusion.8
  117.1 16.4 %all-gather.12 = f16[384,2048]{1,0:T(8,128)(2,1)S(1)} all-gather(f16[48,2048]{1,0:T(8,128)(2,1)S(1)} %multiply_convert_fusion.8), channel_id=1, replica_groups=mesh['z'=16,'y'=4,'x'=4,'c'=2] {'x','c'}, dimensions={0}, use_global_device_ids=true | all-gather | bytes 1769472 | tf_op jit(solution)/shard_map/all_gather | solution.py:100
  133.5 0.0 all-gather.9.cloned.1.call-done
  133.5 0.0 copy-start.1
  133.5 2.5 %fusion.5 = f32[384,384]{1,0:T(8,128)S(1)} fusion(bf16[2048,1152]{1,0:T(8,128)(2,1)} %all-gather.9.cloned.1.call-done, f16[384,2048]{1,0:T(8,128)(2,1)S(1)} %all-gather.12), kind=kOutput, calls=%fused_computation.11 | convolution fusion | flops 606339072 | bytes 3735552 | tf_op jit(solution)/shard_map/dot_general | solution.py:58
  136.0 0.3 copy-done.1
  136.3 1.0 fusion.30
  137.3 0.7 convolution_convert_fusion
  138.1 2.1 %collective-permute-start.1 = (bf16[192,2048]{1,0:T(8,128)(2,1)S(1)}, bf16[192,2048]{1,0:T(8,128)(2,1)S(1)}, u32[]{:S(2)}, u32[]{:S(2)}) collective-permute-start(bf16[192,2048]{1,0:T(8,128)(2,1)S(1)} %convolution_convert_fusion), channel_id=1, source_target_pairs={{0,1},{1,0},{2,3},{3,2},{4,5},{5,4},{6,7},{7,6},{8,9},{9,8},{10,11... | collective-permute-start | bytes 2359304 | tf_op jit(solution)/shard_map/ppermute | solution.py:22
  140.1 2.1 %collective-permute-done.1 = bf16[192,2048]{1,0:T(8,128)(2,1)S(1)} collective-permute-done((bf16[192,2048]{1,0:T(8,128)(2,1)S(1)}, bf16[192,2048]{1,0:T(8,128)(2,1)S(1)}, u32[]{:S(2)}, u32[]{:S(2)}) %collective-permute-start.1) | collective-permute-done | bytes 786464 | tf_op jit(solution)/shard_map/ppermute | solution.py:22
  142.2 0.7 add_convert_fusion
  143.0 14.5 %all_to_all.11 = bf16[4,48,2048]{2,1,0:T(8,128)(2,1)S(1)} all-to-all(bf16[4,48,2048]{2,1,0:T(8,128)(2,1)S(1)} %bitcast.32), channel_id=1, replica_groups=mesh['z'=16,'y'=4,'x'=4,'c'=2] {'x'}, dimensions={0} | all-to-all | bytes 1572864 | tf_op jit(solution)/shard_map/all_to_all | solution.py:74
  157.5 0.1 convert_reduce_fusion
  157.6 10.9 %all-gather = bf16[192,2048]{1,0:T(8,128)(2,1)S(1)} all-gather(bf16[48,2048]{1,0:T(8,128)(2,1)S(1)} %add_convert_fusion.2), channel_id=2, replica_groups=mesh['z'=16,'y'=4,'x'=4,'c'=2] {'x'}, dimensions={0}, use_global_device_ids=true | all-gather | bytes 983040 | tf_op jit(solution)/shard_map/all_gather | solution.py:105
  168.6 6.3 %collective-permute-start.2 = (bf16[4,48,2048]{2,1,0:T(8,128)(2,1)S(1)}, bf16[4,48,2048]{2,1,0:T(8,128)(2,1)S(1)}, u32[]{:S(2)}, u32[]{:S(2)}) collective-permute-start(bf16[4,48,2048]{2,1,0:T(8,128)(2,1)S(1)} %bitcast.33), channel_id=1, source_target_pairs={{0,1},{1,0},{2,3},{3,2},{4,5},{5,4},{6,7},{7,6},{8,9},{9,8},{10,11... | collective-permute-start | bytes 2359304 | tf_op jit(solution)/shard_map/ppermute | solution.py:22
  174.9 1.9 %collective-permute-done.2 = bf16[4,48,2048]{2,1,0:T(8,128)(2,1)S(1)} collective-permute-done((bf16[4,48,2048]{2,1,0:T(8,128)(2,1)S(1)}, bf16[4,48,2048]{2,1,0:T(8,128)(2,1)S(1)}, u32[]{:S(2)}, u32[]{:S(2)}) %collective-permute-start.2) | collective-permute-done | bytes 786464 | tf_op jit(solution)/shard_map/ppermute | solution.py:22
  176.8 0.1 select_bitcast_fusion.1
  176.9 1.3 pad_maximum_fusion
  (5 shorter events, 0.1 us)
Async XLA Ops:
  6.5 41.9 %copy-start = (bf16[384,2048]{1,0:T(8,128)(2,1)S(1)}, bf16[384,2048]{1,0:T(8,128)(2,1)}, u32[]{:S(2)}) copy-start(bf16[384,2048]{1,0:T(8,128)(2,1)} %param.10) | copy-start | bytes 4718596
  6.5 40.2 %all-gather.7.cloned.1.call-start = ((), (), s32[]{:S(2)}) async-start(), calls=%async_computation.2 | async-start | bytes 1474560 | tf_op jit(solution)/shard_map/all_gather | solution.py:42
  9.0 124.5 %all-gather.9.cloned.1.call-start = ((), (), s32[]{:S(2)}) async-start(), calls=%async_computation.3 | async-start | bytes 5013504 | tf_op jit(solution)/shard_map/all_gather | solution.py:47
  84.2 1.2 copy-start.3
  88.3 11.3 %collective-permute-start = (bf16[192,2048]{1,0:T(8,128)(2,1)S(1)}, bf16[192,2048]{1,0:T(8,128)(2,1)S(1)}, u32[]{:S(2)}, u32[]{:S(2)}) collective-permute-start(bf16[192,2048]{1,0:T(8,128)(2,1)S(1)} %convolution_convert_fusion.1), channel_id=1, source_target_pairs={{0,1},{1,0},{2,3},{3,2},{4,5},{5,4},{6,7},{7,6},{8,9},{9,8},{10,11... | collective-permute-start | bytes 2359304 | tf_op jit(solution)/shard_map/ppermute | solution.py:22
  115.6 1.4 copy-start.2
  133.5 2.8 %copy-start.1 = (bf16[2048,1152]{1,0:T(8,128)(2,1)S(1)}, bf16[2048,1152]{1,0:T(8,128)(2,1)}, u32[]{:S(2)}) copy-start(bf16[2048,1152]{1,0:T(8,128)(2,1)} %all-gather.9.cloned.1.call-done) | copy-start | bytes 14155780
  138.1 4.2 %collective-permute-start.1 = (bf16[192,2048]{1,0:T(8,128)(2,1)S(1)}, bf16[192,2048]{1,0:T(8,128)(2,1)S(1)}, u32[]{:S(2)}, u32[]{:S(2)}) collective-permute-start(bf16[192,2048]{1,0:T(8,128)(2,1)S(1)} %convolution_convert_fusion), channel_id=1, source_target_pairs={{0,1},{1,0},{2,3},{3,2},{4,5},{5,4},{6,7},{7,6},{8,9},{9,8},{10,11... | collective-permute-start | bytes 2359304 | tf_op jit(solution)/shard_map/ppermute | solution.py:22
  168.6 8.2 %collective-permute-start.2 = (bf16[4,48,2048]{2,1,0:T(8,128)(2,1)S(1)}, bf16[4,48,2048]{2,1,0:T(8,128)(2,1)S(1)}, u32[]{:S(2)}, u32[]{:S(2)}) collective-permute-start(bf16[4,48,2048]{2,1,0:T(8,128)(2,1)S(1)} %bitcast.33), channel_id=1, source_target_pairs={{0,1},{1,0},{2,3},{3,2},{4,5},{5,4},{6,7},{7,6},{8,9},{9,8},{10,11... | collective-permute-start | bytes 2359304 | tf_op jit(solution)/shard_map/ppermute | solution.py:22
Sparse Core Ops, SparseCore 0:
  9.4 35.3 all-gather.6
  48.6 72.4 all-gather.8

commit v2 on v1

--- a/solution.py
+++ b/solution.py
@@ -37,12 +37,11 @@
 
 def gather_weights(first, second):
     rows, width = second.shape
-    padded = jnp.pad(second, ((0, (NY - 1) * rows), (0, 0)))
-    padded, first = lax.optimization_barrier((padded, first))
-    second_y = lax.all_gather(padded, "y", axis=0, tiled=True)
+    row = lax.broadcasted_iota(jnp.int32, (NY * rows, width), 0)
+    spread = jnp.where(row // rows == lax.axis_index("y"), jnp.tile(second, (NY, 1)), jnp.zeros((), second.dtype))
+    spread, first = lax.optimization_barrier((spread, first))
+    block = lax.psum(spread, "y")
     first_z = lax.all_gather(first, "z", axis=0, tiled=True)
-    second_y, first_z = lax.optimization_barrier((second_y, first_z))
-    block = second_y.reshape(NY, -1, width)[:, :rows].reshape(NY * rows, width)
     block, first_z = lax.optimization_barrier((block, first_z))
     second_whole = lax.all_gather(block, "z", axis=0, tiled=True)
     first_whole = lax.all_gather(first_z.reshape(NZ, rows, width), "y", axis=1, tiled=True)
@@ -78,6 +77,30 @@
     return jnp.sum(pieces.astype(jnp.float32), axis=0)
 
 
+def power_of_two(p):
+    size = jnp.abs(p)
+    out = jnp.ones(p.shape, jnp.float32)
+    for bit in range(7):
+        factor = jnp.where(p < 0, 2.0 ** -(2**bit), 2.0 ** (2**bit))
+        out = jnp.where((size >> bit) & 1 == 1, out * factor, out)
+    return out
+
+
+def spread_rows(finished):
+    share, width = finished.shape
+    wide = finished.astype(jnp.float32)
+    top = jnp.max(jnp.abs(wide), axis=1, keepdims=True)
+    power = jnp.floor(jnp.log2(jnp.maximum(top, 2.0**-100)))
+    power = jnp.clip(power, -100.0, 127.0)
+    coded = wide * power_of_two(13 - power.astype(jnp.int32))
+    tail = jnp.broadcast_to(power, (share, 128))
+    sent = jnp.concatenate([coded, tail], axis=1).astype(jnp.float16)
+    everyone = lax.all_gather(sent, TP, axis=0, tiled=True)
+    back = power_of_two(everyone[:, width : width + 1].astype(jnp.float32).astype(jnp.int32) - 13)
+    everyone, back = lax.optimization_barrier((everyone, back))
+    return (everyone[:, :width].astype(jnp.float32) * back).astype(jnp.bfloat16)
+
+
 def body(tokens, merged, gain_first, gate_first, up_first, down_first, gain_second, gate_second, up_second, down_second):
     rows = tokens.shape[0]
     share = rows // (NX * NC)
@@ -102,11 +125,7 @@
     hidden_two = folded(normed_second, second[0], second[1])
     second_sum = added(pieces_at_owner(hidden_two, second[2], share))
     finished = (middle + 0.5 * second_sum).astype(jnp.bfloat16)
-    mine = lax.all_gather(finished, "x", axis=0)
-    theirs = swap_cores(mine)
-    low = jnp.where(core == 0, mine, theirs)
-    high = jnp.where(core == 0, theirs, mine)
-    return jnp.stack([low, high], axis=1).reshape(rows, -1)
+    return spread_rows(finished)
 
 
 def solution(mesh):

time: 185 us -> 205 us (1.11)
  waiting for transfers between devices: 5.91 us -> 28.4 us
  starting transfers between devices: 17.8 us -> 7.64 us
  blocking collectives: 130 us -> 138 us
  local copies, waits for them, and re-layouts: 2.82 us -> 0.46 us
    psum x0 -> x1, waiting for transfers between devices: none -> 24.4 us  [gather_weights(): block = lax.psum(spread, 'y')]
    ppermute x3 -> x2, starting transfers between devices: 17.8 us -> 7.59 us  [swap_cores(): return lax.ppermute(x, 'c', [(0, 1), (1, 0)])]
    all_gather x1, blocking collectives: 10.9 us -> 16.6 us  [spread_rows(): everyone = lax.all_gather(sent, TP, axis=0, tiled=True)]
    all_gather x1, blocking collectives: 35.4 us -> 39.3 us  [gather_weights(): lax.all_gather(first_z.reshape(NZ, rows, width), 'y', axis=1, tiled=True)]
    ppermute x3 -> x2, waiting for transfers between devices: 5.88 us -> 3.99 us  [swap_cores(): return lax.ppermute(x, 'c', [(0, 1), (1, 0)])]
  transfers between devices with their start and end apart: 5 -> 4, of which waited for: 3 -> 3; matrix products, arithmetic and copies ran while one was open for 4% -> 3% of each run, Pallas kernels for 0% -> 0%
where the time goes in v2:
time: 205 us
  blocking collectives  138 us (67%)
  waiting for transfers between devices  28.4 us (14%)
  between operations  13.6 us (7%)
  matrix products  8.47 us (4%)
  other arithmetic  8.05 us (4%)
  starting transfers between devices  7.64 us (4%)
    all_gather x1, blocking collectives, gather_weights(): lax.all_gather(first_z.reshape(NZ, rows, width), 'y', axis=1, tiled=True)  39.3 us
    all_gather x1, blocking collectives, gather_weights(): first_z = lax.all_gather(first, 'z', axis=0, tiled=True)  36.8 us
    all_to_all x2, blocking collectives, pieces_at_owner(): return lax.all_to_all(chip.reshape(NX, share, -1), 'x', 0, 0, tiled=True)  29.5 us
    psum x1, waiting for transfers between devices, gather_weights(): block = lax.psum(spread, 'y')  24.4 us
    all_gather x1, blocking collectives, spread_rows(): everyone = lax.all_gather(sent, TP, axis=0, tiled=True)  16.6 us
    all_gather x1, blocking collectives, body(): everyone = lax.all_gather(coded, TP, axis=0, tiled=True)  16.3 us
    ppermute x2, starting transfers between devices, swap_cores(): return lax.ppermute(x, 'c', [(0, 1), (1, 0)])  7.59 us
  transfers between devices with their start and end apart: 4, of which 3 were waited for; matrix products, arithmetic and copies ran while one was open for 3% of the time, Pallas kernels for 0%

profile of v2, /device:TPU:1, one launch (start us, length us, event | category | flops | bytes accessed | tf_op | source)
XLA Modules:
  0.0 205.0 jit_solution(1046176522694820344)
XLA Ops:
  6.5 0.0 copy-start
  6.5 0.0 all-reduce.8.cloned.1.call-start
  6.6 0.9 fusion.48
  7.5 0.8 multiply_convert_fusion.11
  8.3 0.8 fusion.33
  9.1 0.0 all-reduce.8.cloned.1.call-update
  9.1 0.0 all-gather.6.cloned.1.call-start
  9.2 36.8 %all-gather.7 = f16[512,1152]{1,0:T(8,128)(2,1)S(1)} all-gather(f16[32,1152]{1,0:T(8,128)(2,1)S(1)} %multiply_convert_fusion.11), channel_id=1, replica_groups=mesh['z'=16,'y'=4,'x'=4,'c'=2] {'z'}, dimensions={0}, use_global_device_ids=true | all-gather | bytes 1253376 | tf_op jit(solution)/shard_map/all_gather | solution.py:44
  45.9 24.4 %all-reduce.8.cloned.1.call-done = bf16[128,1152]{1,0:T(8,128)(2,1)} async-done(((bf16[128,1152]{1,0:T(8,128)(2,1)}), bf16[128,1152]{1,0:T(8,128)(2,1)}) %all-reduce.8.cloned.1.call-update) | async-done | bytes 294928 | tf_op jit(solution)/shard_map/psum | solution.py:43
  70.3 0.0 all-gather.6.cloned.1.call-update
  70.3 0.0 copy-done
  70.3 0.4 fusion
  70.7 39.3 %all-gather.8 = f16[16,128,1152]{2,1,0:T(8,128)(2,1)S(1)} all-gather(f16[16,32,1152]{2,1,0:T(8,128)(2,1)S(1)} %bitcast.22), channel_id=1, replica_groups=mesh['z'=16,'y'=4,'x'=4,'c'=2] {'y'}, dimensions={1}, use_global_device_ids=true | all-gather | bytes 5898240 | tf_op jit(solution)/shard_map/all_gather | solution.py:47
  110.0 0.0 copy-start.3
  110.0 1.2 multiply_convert_fusion
  111.2 0.0 copy-done.3
  111.2 1.0 fusion.9
  112.3 1.0 fusion.27
  113.4 0.7 convolution_convert_fusion.1
  114.1 5.5 %collective-permute-start = (bf16[192,2048]{1,0:T(8,128)(2,1)S(1)}, bf16[192,2048]{1,0:T(8,128)(2,1)S(1)}, u32[]{:S(2)}, u32[]{:S(2)}) collective-permute-start(bf16[192,2048]{1,0:T(8,128)(2,1)S(1)} %convolution_convert_fusion.1), channel_id=1, source_target_pairs={{0,1},{1,0},{2,3},{3,2},{4,5},{5,4},{6,7},{7,6},{8,9},{9,8},{10,11... | collective-permute-start | bytes 2359304 | tf_op jit(solution)/shard_map/ppermute | solution.py:22
  119.6 1.9 collective-permute-done
  121.5 0.7 add_convert_fusion.1
  122.2 15.3 %all_to_all.10 = bf16[4,48,2048]{2,1,0:T(8,128)(2,1)S(1)} all-to-all(bf16[4,48,2048]{2,1,0:T(8,128)(2,1)S(1)} %bitcast.23), channel_id=1, replica_groups=mesh['z'=16,'y'=4,'x'=4,'c'=2] {'x'}, dimensions={0} | all-to-all | bytes 1572864 | tf_op jit(solution)/shard_map/all_to_all | solution.py:73
  137.5 0.0 copy-start.2
  137.5 0.1 convert_reduce_fusion.1
  137.6 1.2 multiply_reduce_fusion
  138.8 0.0 copy-done.2
  138.8 0.1 multiply_convert_fusion.9
  139.0 16.3 %all-gather.9 = f16[384,2048]{1,0:T(8,128)(2,1)S(1)} all-gather(f16[48,2048]{1,0:T(8,128)(2,1)S(1)} %multiply_convert_fusion.9), channel_id=1, replica_groups=mesh['z'=16,'y'=4,'x'=4,'c'=2] {'x','c'}, dimensions={0}, use_global_device_ids=true | all-gather | bytes 1769472 | tf_op jit(solution)/shard_map/all_gather | solution.py:123
  155.2 0.0 all-gather.6.cloned.1.call-done
  155.2 0.0 copy-start.1
  155.2 2.5 %fusion.5 = f32[384,384]{1,0:T(8,128)S(1)} fusion(bf16[2048,1152]{1,0:T(8,128)(2,1)} %all-gather.6.cloned.1.call-done, f16[384,2048]{1,0:T(8,128)(2,1)S(1)} %all-gather.9), kind=kOutput, calls=%fused_computation.12 | convolution fusion | flops 606339072 | bytes 3735552 | tf_op jit(solution)/shard_map/dot_general | solution.py:57
  157.8 0.3 copy-done.1
  158.1 1.0 fusion.30
  159.1 0.7 convolution_convert_fusion
  159.8 2.1 %collective-permute-start.1 = (bf16[192,2048]{1,0:T(8,128)(2,1)S(1)}, bf16[192,2048]{1,0:T(8,128)(2,1)S(1)}, u32[]{:S(2)}, u32[]{:S(2)}) collective-permute-start(bf16[192,2048]{1,0:T(8,128)(2,1)S(1)} %convolution_convert_fusion), channel_id=1, source_target_pairs={{0,1},{1,0},{2,3},{3,2},{4,5},{5,4},{6,7},{7,6},{8,9},{9,8},{10,11... | collective-permute-start | bytes 2359304 | tf_op jit(solution)/shard_map/ppermute | solution.py:22
  161.9 2.1 %collective-permute-done.1 = bf16[192,2048]{1,0:T(8,128)(2,1)S(1)} collective-permute-done((bf16[192,2048]{1,0:T(8,128)(2,1)S(1)}, bf16[192,2048]{1,0:T(8,128)(2,1)S(1)}, u32[]{:S(2)}, u32[]{:S(2)}) %collective-permute-start.1) | collective-permute-done | bytes 786464 | tf_op jit(solution)/shard_map/ppermute | solution.py:22
  164.0 0.7 add_convert_fusion
  164.8 14.3 %all_to_all.11 = bf16[4,48,2048]{2,1,0:T(8,128)(2,1)S(1)} all-to-all(bf16[4,48,2048]{2,1,0:T(8,128)(2,1)S(1)} %bitcast.24), channel_id=1, replica_groups=mesh['z'=16,'y'=4,'x'=4,'c'=2] {'x'}, dimensions={0} | all-to-all | bytes 1572864 | tf_op jit(solution)/shard_map/all_to_all | solution.py:73
  179.0 0.1 convert_reduce_fusion
  179.1 0.2 fusion.36
  179.3 0.1 fusion.37
  179.5 0.1 broadcast_in_dim.124
  179.5 0.1 pad_maximum_fusion
  179.6 16.6 %all-gather.10 = f16[384,2176]{1,0:T(8,128)(2,1)S(1)} all-gather(f16[48,2176]{1,0:T(8,128)(2,1)S(1)} %pad_maximum_fusion), channel_id=1, replica_groups=mesh['z'=16,'y'=4,'x'=4,'c'=2] {'x','c'}, dimensions={0}, use_global_device_ids=true | all-gather | bytes 1880064 | tf_op jit(solution)/shard_map/all_gather | solution.py:98
  196.2 0.3 multiply_select_fusion
  196.5 0.1 reduce
  196.6 1.5 multiply_convert_fusion.1
  (7 shorter events, 0.1 us)
Async XLA Ops:
  6.5 63.8 %copy-start = (bf16[384,2048]{1,0:T(8,128)(2,1)S(1)}, bf16[384,2048]{1,0:T(8,128)(2,1)}, u32[]{:S(2)}) copy-start(bf16[384,2048]{1,0:T(8,128)(2,1)} %param.10) | copy-start | bytes 4718596
  6.5 63.7 %all-reduce.8.cloned.1.call-start = ((), (), s32[]{:S(2)}) async-start(), calls=%async_computation.2 | async-start | bytes 589824 | tf_op jit(solution)/shard_map/psum | solution.py:43
  9.1 146.1 %all-gather.6.cloned.1.call-start = ((), (), s32[]{:S(2)}) async-start(), calls=%async_computation.3 | async-start | bytes 5013504 | tf_op jit(solution)/shard_map/all_gather | solution.py:46
  110.0 1.2 copy-start.3
  114.1 7.4 %collective-permute-start = (bf16[192,2048]{1,0:T(8,128)(2,1)S(1)}, bf16[192,2048]{1,0:T(8,128)(2,1)S(1)}, u32[]{:S(2)}, u32[]{:S(2)}) collective-permute-start(bf16[192,2048]{1,0:T(8,128)(2,1)S(1)} %convolution_convert_fusion.1), channel_id=1, source_target_pairs={{0,1},{1,0},{2,3},{3,2},{4,5},{5,4},{6,7},{7,6},{8,9},{9,8},{10,11... | collective-permute-start | bytes 2359304 | tf_op jit(solution)/shard_map/ppermute | solution.py:22
  137.5 1.4 copy-start.2
  155.2 2.8 %copy-start.1 = (bf16[2048,1152]{1,0:T(8,128)(2,1)S(1)}, bf16[2048,1152]{1,0:T(8,128)(2,1)}, u32[]{:S(2)}) copy-start(bf16[2048,1152]{1,0:T(8,128)(2,1)} %all-gather.6.cloned.1.call-done) | copy-start | bytes 14155780
  159.8 4.2 %collective-permute-start.1 = (bf16[192,2048]{1,0:T(8,128)(2,1)S(1)}, bf16[192,2048]{1,0:T(8,128)(2,1)S(1)}, u32[]{:S(2)}, u32[]{:S(2)}) collective-permute-start(bf16[192,2048]{1,0:T(8,128)(2,1)S(1)} %convolution_convert_fusion), channel_id=1, source_target_pairs={{0,1},{1,0},{2,3},{3,2},{4,5},{5,4},{6,7},{7,6},{8,9},{9,8},{10,11... | collective-permute-start | bytes 2359304 | tf_op jit(solution)/shard_map/ppermute | solution.py:22
Sparse Core Ops, SparseCore 0:
  9.7 60.5 all-reduce.7
  72.4 73.4 all-gather.5
